TPU v7x, 32 devices: a whole 2x2x4 slice. The times are simulated.
32 devices in a mesh: sp: 16 (over z, y, x), tp: 2 (over core).
Axes of the slice: x: 2, y: 2, z: 4, core: 2. Of those that a mesh axis runs over, the one named last changes fastest.
Arguments:
- tokens_in: bfloat16 [2048, 2048], P(('sp', 'tp')), may hold values from -9 to 9, as said below
- w_query: bfloat16 [2048, 2048], P(None, 'tp'), may hold values from -0.125 to 0.125
- w_key: bfloat16 [2048, 512], P(None, 'tp'), may hold values from -0.125 to 0.125
- w_value: bfloat16 [2048, 512], P(None, 'tp'), may hold values from -0.125 to 0.125
- w_out: bfloat16 [2048, 2048], P('tp'), may hold values from -0.125 to 0.125
- q_gain: float32 [64], replicated, may hold values from 0.1 to 14
- k_gain: float32 [64], replicated, may hold values from 0.1 to 14
Outputs:
- attended: bfloat16 [2048, 2048], P(('sp', 'tp'))
Inputs may be any that keep to these rules, and one draw needn't show every extreme that they name: `tokens_in`: activations whose mean differs from one block of 128 tokens to another.
All inputs are finite; a program needn't handle non-finite values.
Results may differ from a plain program's by a relative error of at most 0.014.
The roundings to bfloat16 on the way count: a program that leaves them out, or rounds other values in their place, can miss the bound.
Values may be sent and summed in bfloat16 or wider, within the bound.
A program may use at most 64 MiB of HBM per device.

v0:
```python
import jax
import jax.numpy as jnp
from jax import lax
from jax.sharding import PartitionSpec as P

GRID_W = 64


def turned(vectors, position, gain):
    pairs = vectors.shape[-1] // 4
    scaled = vectors * lax.rsqrt(jnp.mean(vectors * vectors, axis=-1, keepdims=True) + 1e-06) * gain
    freq = 10000.0 ** (-jnp.arange(pairs, dtype=jnp.float32) / pairs)
    grid_row = (position // GRID_W).astype(jnp.float32)
    grid_col = (position % GRID_W).astype(jnp.float32)
    angle = jnp.stack([grid_row[:, None] * freq, grid_col[:, None] * freq], axis=1)
    cosine = jnp.cos(angle)[:, None]
    sine = jnp.sin(angle)[:, None]
    split = scaled.reshape(scaled.shape[:-1] + (2, 2, pairs))
    first = split[..., 0, :]
    second = split[..., 1, :]
    joined = jnp.stack([first * cosine - second * sine, first * sine + second * cosine], axis=-2)
    return joined.reshape(scaled.shape)


def body(tokens_in, w_query, w_key, w_value, w_out, q_gain, k_gain):
    head_dim = q_gain.shape[0]
    query_cols = w_query.shape[1]
    key_cols = w_key.shape[1]
    kv_heads = key_cols // head_dim
    group = query_cols // key_cols
    w_joined = jnp.concatenate([w_query, w_key, w_value], axis=1)
    projected = jnp.dot(
        lax.all_gather(tokens_in, "tp", axis=0, tiled=True),
        w_joined,
        preferred_element_type=jnp.float32,
    ).astype(jnp.bfloat16)
    row_count = projected.shape[0]
    position = lax.axis_index("sp") * row_count + jnp.arange(row_count, dtype=jnp.int32)
    query_n = turned(
        projected[:, :query_cols]
        .astype(jnp.float32)
        .reshape(row_count, kv_heads * group, head_dim),
        position,
        q_gain,
    ).astype(jnp.bfloat16)
    query_g = query_n.reshape(row_count, kv_heads, group, head_dim).transpose(1, 2, 0, 3)
    raw_keys = projected[:, query_cols : query_cols + key_cols]
    values = projected[:, query_cols + key_cols :]
    scale = head_dim ** (-0.5)
    outgoing = jnp.concatenate([raw_keys, values], axis=1)
    piece = lax.all_gather(outgoing, "sp", axis=0, tiled=True)
    length = piece.shape[0]
    spot = jnp.arange(length, dtype=jnp.int32)
    keys_n = turned(
        piece[:, :key_cols].astype(jnp.float32).reshape(length, kv_heads, head_dim), spot, k_gain
    ).astype(jnp.bfloat16)
    peak = jnp.full((kv_heads, group, row_count), -1e30, jnp.float32)
    scores = (
        jnp.einsum("kgqd,nkd->kgqn", query_g, keys_n, preferred_element_type=jnp.float32) * scale
    )
    new_peak = jnp.maximum(peak, jnp.max(scores, axis=-1))
    expo = jnp.exp(scores - new_peak[..., None])
    total = jnp.sum(expo, axis=-1)
    summed = jnp.einsum(
        "kgqn,nkd->kgqd",
        expo.astype(jnp.bfloat16),
        piece[:, key_cols:].reshape(length, kv_heads, head_dim),
        preferred_element_type=jnp.float32,
    )
    peak, total, summed = (new_peak, total, summed)
    mixed = (summed / total[..., None]).astype(jnp.bfloat16)
    mixed = mixed.transpose(2, 0, 1, 3).reshape(row_count, query_cols)
    return lax.psum_scatter(
        jnp.dot(mixed, w_out, preferred_element_type=jnp.float32).astype(jnp.bfloat16),
        "tp",
        scatter_dimension=0,
        tiled=True,
    )


def solution(mesh):
    return jax.shard_map(
        body,
        mesh=mesh,
        in_specs=(
            P(("sp", "tp"), None),
            P(None, "tp"),
            P(None, "tp"),
            P(None, "tp"),
            P("tp", None),
            P(),
            P(),
        ),
        out_specs=P(("sp", "tp"), None),
        check_vma=False,
    )
```

profile of v0, /device:TPU:0, one launch (start us, length us, event | category | flops | bytes accessed | tf_op | source)
XLA Modules:
  0.0 117.6 jit_solution(13708748384121845471)
XLA Ops:
  6.5 0.0 all-gather.2.cloned.1.call-start
  6.5 2.5 %all_gather.6 = bf16[128,2048]{1,0:T(8,128)(2,1)S(1)} all-gather(bf16[64,2048]{1,0:T(8,128)(2,1)} %param.7), channel_id=1, replica_groups=mesh['sp'=16,'tp'=2] {'tp'}, dimensions={0}, use_global_device_ids=true | all-gather | bytes 786432 | tf_op jit(solution)/shard_map/all_gather | solution.py:33
  9.0 0.0 copy-start.1
  9.0 0.0 copy-start.2
  9.0 4.1 %fusion.13 = bf16[128,1536]{0,1:T(8,128)(2,1)S(1)} fusion(bf16[128,2048]{1,0:T(8,128)(2,1)S(1)} %all_gather.6, bf16[2048,256]{1,0:T(8,128)(2,1)} %param.10, bf16[2048,256]{1,0:T(8,128)(2,1)} %param.9, bf16[2048,1024]{1,0:T(8,128)(2,1)} %param.8), kind=kOutput, calls=%fused_computation.13 | convolution fusion | flops 824377344 | bytes 7208960 | tf_op jit(solution)/shard_map/dot_general | solution.py:32
  13.1 0.7 concatenate.24
  13.8 0.0 all-gather.2.cloned.1.call-update
  13.8 0.0 reduce-scatter.2.cloned.1.call-start
  13.8 0.0 copy-done.1
  13.9 0.1 mul.221
  13.9 0.0 copy-done.2
  13.9 0.1 mul.240
  14.1 0.1 broadcast_multiply_fusion.3
  14.1 0.1 fusion.34
  14.2 0.1 bitcast_reduce_fusion.1
  14.4 0.1 multiply_multiply_fusion.1
  14.5 0.1 subtract_convert_fusion.1
  14.6 0.1 broadcast_multiply_fusion.1
  14.7 1.0 fusion.27
  15.7 63.8 %all-gather.2.cloned.1.call-done = bf16[2048,512]{0,1:T(8,128)(2,1)} async-done(((bf16[128,512]{0,1:T(8,128)(2,1)}), bf16[2048,512]{0,1:T(8,128)(2,1)}) %all-gather.2.cloned.1.call-update) | async-done | bytes 2097168 | tf_op jit(solution)/shard_map/all_gather | solution.py:51
  79.5 1.5 %bitcast_reduce_fusion = f32[2048,4]{0,1:T(4,128)S(1)} fusion(bf16[2048,512]{0,1:T(8,128)(2,1)} %all-gather.2.cloned.1.call-done), kind=kLoop, calls=%fused_computation.14 | loop fusion | flops 1564672 | bytes 1081344 | tf_op jit(solution)/shard_map/reduce_sum | solution.py:11
  81.0 1.8 %slice_convert_fusion = (f32[2048,256]{0,1:T(8,128)S(1)}, bf16[2048,256]{0,1:T(8,128)(2,1)S(1)}) fusion(bf16[2048,512]{0,1:T(8,128)(2,1)} %all-gather.2.cloned.1.call-done), kind=kLoop, calls=%fused_computation.17 | loop fusion | flops 524288 | bytes 5242880 | tf_op jit(solution)/shard_map/convert_element_type | solution.py:55
  82.9 0.4 multiply_multiply_fusion
  83.3 0.3 subtract_convert_fusion
  83.6 0.1 pad_maximum_fusion
  83.7 2.5 %multiply_reduce_fusion = (f32[4,4,128]{2,1,0:T(4,128)S(1)}, f32[4,4,128,2048]{3,2,1,0:T(8,128)S(1)}) fusion(bf16[4,4,128,64]{2,3,1,0:T(8,128)(2,1)S(1)} %bitcast.38, bf16[2048,4,64,1]{0,2,3,1:T(8,128)(2,1)S(1)} %bitcast.36), kind=kOutput, calls=%fused_computation.1 | convolution fusion | flops 545257472 | bytes 18096128 | tf_op jit(solution)/shard_map/kgqd,nkd->kgqn/dot_general | solution.py:59
  86.2 3.3 %fusion = f32[4,4,128]{2,1,0:T(4,128)S(1)} fusion(f32[4,4,128,2048]{3,2,1,0:T(8,128)S(1)} %get-tuple-element.20, f32[4,4,128]{2,1,0:T(4,128)S(1)} %broadcast_maximum_fusion), kind=kLoop, calls=%fused_computation.2 | loop fusion | flops 12580864 | bytes 16793600 | tf_op jit(solution)/shard_map/reduce_sum | solution.py:63
  89.5 2.4 %copy-done = f32[4,4,128,2048]{3,2,1,0:T(8,128)} copy-done((f32[4,4,128,2048]{3,2,1,0:T(8,128)}, f32[4,4,128,2048]{3,2,1,0:T(8,128)S(1)}, u32[]{:S(2)}) %copy-start) | copy-done | bytes 16777240
  91.9 8.8 %fusion.22 = bf16[128,4,4,64]{0,3,2,1:T(8,128)(2,1)S(1)} fusion(bf16[2048,4,64,1]{0,2,3,1:T(8,128)(2,1)S(1)} %bitcast.39, f32[4,4,128,2048]{3,2,1,0:T(8,128)} %copy-done, f32[4,4,128]{2,1,0:T(4,128)S(1)} %broadcast_maximum_fusion, f32[128,4,4]{0,2,1:T(4,128)S(1)} %bitcast.41), kind=kOutput, calls=%fused_computation.22 | convolution fusion | flops 549715968 | bytes 18104320 | tf_op jit(solution)/shard_map/kgqn,nkd->kgqd/dot_general | solution.py:64
  100.8 3.7 %convolution_convert_fusion = bf16[128,2048]{1,0:T(8,128)(2,1)} fusion(bf16[128,1024]{0,1:T(8,128)(2,1)S(1)} %bitcast.40, bf16[1024,2048]{1,0:T(8,128)(2,1)} %param.11), kind=kOutput, calls=%fused_computation.12 | convolution fusion | flops 537133056 | bytes 4980736 | tf_op jit(solution)/shard_map/dot_general | solution.py:74
  104.5 0.0 reduce-scatter.2.cloned.1.call-update
  104.5 6.3 %reduce-scatter.2.cloned.1.call-done = bf16[64,2048]{1,0:T(8,128)(2,1)} async-done(((bf16[128,2048]{1,0:T(8,128)(2,1)}), bf16[64,2048]{1,0:T(8,128)(2,1)}) %reduce-scatter.2.cloned.1.call-update) | async-done | bytes 262160 | tf_op jit(solution)/shard_map/reduce_scatter | solution.py:73
  (9 shorter events, 0.1 us)
Async XLA Ops:
  6.5 73.0 %all-gather.2.cloned.1.call-start = ((), (), s32[]{:S(2)}) async-start(), calls=%async_computation.1 | async-start | bytes 2228224 | tf_op jit(solution)/shard_map/all_gather | solution.py:51
  9.0 4.8 %copy-start.1 = (f32[64]{0:T(128)S(1)}, f32[64]{0:T(128)}, u32[]{:S(2)}) copy-start(f32[64]{0:T(128)} %param.12) | copy-start | bytes 772
  9.0 4.9 %copy-start.2 = (f32[64]{0:T(128)S(1)}, f32[64]{0:T(128)}, u32[]{:S(2)}) copy-start(f32[64]{0:T(128)} %param.13) | copy-start | bytes 772
  13.8 97.0 %reduce-scatter.2.cloned.1.call-start = ((), (), s32[]{:S(2)}) async-start(), calls=%async_computation.2 | async-start | bytes 786432 | tf_op jit(solution)/shard_map/reduce_scatter | solution.py:73
  86.2 5.7 %copy-start = (f32[4,4,128,2048]{3,2,1,0:T(8,128)}, f32[4,4,128,2048]{3,2,1,0:T(8,128)S(1)}, u32[]{:S(2)}) copy-start(f32[4,4,128,2048]{3,2,1,0:T(8,128)S(1)} %get-tuple-element.20) | copy-start | bytes 50331652
Sparse Core Ops, SparseCore 0:
  13.9 65.5 all-gather.1
  104.6 6.0 reduce-scatter.1
where the time goes:
time: 118 us
  waiting for transfers between devices  70.1 us (59%)
  matrix products  19.1 us (16%)
  between operations  13.6 us (12%)
  other arithmetic  9.04 us (8%)
  local copies, waits for them, and re-layouts  3.27 us (3%)
  blocking collectives  2.5 us (2%)
    all_gather x1, waiting for transfers between devices, body(): piece = lax.all_gather(outgoing, 'sp', axis=0, tiled=True)  63.8 us
    dot_general x1, matrix products, body(): jnp.einsum('kgqn,nkd->kgqd', expo.astype(jnp.bfloat16), piece[:, key_cols...  8.83 us
    reduce_scatter x1, waiting for transfers between devices, body(): lax.psum_scatter(jnp.dot(mixed, w_out, preferred_element_type=jnp.float32...  6.26 us
    dot_general x1, matrix products, body(): jnp.dot(lax.all_gather(tokens_in, 'tp', axis=0, tiled=True), w_joined, pr...  4.06 us
    dot_general x1, matrix products, body(): jnp.dot(mixed, w_out, preferred_element_type=jnp.float32)  3.73 us
    reduce_sum x1, other arithmetic, body(): total = jnp.sum(expo, axis=-1)  3.27 us
    all_gather x1, blocking collectives, body(): lax.all_gather(tokens_in, 'tp', axis=0, tiled=True)  2.5 us
    dot_general x1, matrix products, body(): jnp.einsum('kgqd,nkd->kgqn', query_g, keys_n, preferred_element_type=jnp....  2.47 us
  transfers between devices with their start and end apart: 2, of which 2 were waited for; matrix products, arithmetic and copies ran while one was open for 1% of the time, Pallas kernels for 0%

commit v1 on v0

v1 whole, which is shorter than its diff:
```python
import functools

import jax
import jax.numpy as jnp
import numpy as np
from jax import lax
from jax.experimental import pallas as pl
from jax.experimental.pallas import tpu as pltpu
from jax.sharding import PartitionSpec as P

GRID_W = 64
LANES = 128


def tables(token_count, head_dim):
    pairs = head_dim // 4
    lane = np.arange(LANES)
    freq = 10000.0 ** (-(lane % pairs) / pairs)
    sign = np.where(lane % (2 * pairs) < pairs, -1.0, 1.0)

    def both(count):
        angle = np.arange(count)[:, None] * freq[None, :]
        return np.concatenate([np.cos(angle), np.sin(angle) * sign], axis=1).astype(np.float32)

    return both(token_count // GRID_W), both(GRID_W)


def kernel(
    n_sp, n_tp, members, head_dim,
    tok_hbm, wq_hbm, wkv_hbms, wo_hbm, row_ref, col_ref, qg_ref, kg_ref, out_ref,
    x, wq, wkvs, wo, kv_out, kv_all, q_out, q_all, qm, k4, v1, peak, acc, m_out, m_all, o_acc, o_out, o_in,
    load_sem, x_send, x_recv, kv_send, kv_recv, q_send, q_recv, m_send, m_recv, o_send, o_recv,
):
    sp, tp = lax.axis_index("sp"), lax.axis_index("tp")
    own_rows = tok_hbm.shape[0]
    rows = own_rows * n_tp
    groups = n_sp // members
    plane, member = sp // members, sp % members
    query_cols = wq.shape[1]
    width = query_cols // members
    heads = width // head_dim
    first = plane * members

    def sp_copy(src, dst, send, recv, to):
        return pltpu.make_async_remote_copy(
            src_ref=src, dst_ref=dst, send_sem=send, recv_sem=recv,
            device_id={"sp": to}, device_id_type=pl.DeviceIdType.MESH)

    def tp_copy(src, dst, send, recv, to):
        return pltpu.make_async_remote_copy(
            src_ref=src, dst_ref=dst, send_sem=send, recv_sem=recv,
            device_id={"tp": to}, device_id_type=pl.DeviceIdType.MESH)

    def own_slice(index):
        return pl.ds(pl.multiple_of(index * own_rows, own_rows), own_rows)

    loads = [pltpu.make_async_copy(tok_hbm, x.at[own_slice(tp)], load_sem.at[0])]
    for i, (src, dst) in enumerate(zip((*wkv_hbms, wq_hbm, wo_hbm), (*wkvs, wq, wo))):
        loads.append(pltpu.make_async_copy(src, dst, load_sem.at[i + 1]))
    for load in loads:
        load.start()
    barrier = pltpu.get_barrier_semaphore()
    for step in range(1, n_tp):
        pl.semaphore_signal(barrier, inc=1, device_id={"tp": (tp + step) % n_tp}, device_id_type=pl.DeviceIdType.MESH)

    def greet(step, carry):
        pl.semaphore_signal(barrier, inc=1, device_id={"sp": (sp + step) % n_sp}, device_id_type=pl.DeviceIdType.MESH)
        return carry

    lax.fori_loop(1, n_sp, greet, 0)

    lane = lax.broadcasted_iota(jnp.int32, (rows, LANES), 1)
    low = lane % head_dim < head_dim // 2
    left = lane % (head_dim // 2) < head_dim // 4
    even = lane < head_dim
    cos_parts, sin_parts = [], []
    per_dev = rows // GRID_W
    low_g = low[:GRID_W]
    for i in range(per_dev):
        line = row_ref[pl.ds(sp * per_dev + i, 1), :]
        cos_parts.append(jnp.where(low_g, jnp.broadcast_to(line[:, :LANES], (GRID_W, LANES)), col_ref[:, :LANES]))
        sin_parts.append(jnp.where(low_g, jnp.broadcast_to(line[:, LANES:], (GRID_W, LANES)), col_ref[:, LANES:]))
    cosine = jnp.concatenate(cos_parts, axis=0)
    sine = jnp.concatenate(sin_parts, axis=0)
    ones_r = lax.broadcasted_iota(jnp.int32, (LANES, LANES), 0) // head_dim
    ones_c = lax.broadcasted_iota(jnp.int32, (LANES, LANES), 1) // head_dim
    block = jnp.where(ones_r == ones_c, 1.0, 0.0).astype(jnp.bfloat16)
    gain_q = jnp.concatenate([qg_ref[...]] * (LANES // head_dim), axis=1) * head_dim ** (-0.5)
    gain_k = jnp.concatenate([kg_ref[...]] * (LANES // head_dim), axis=1)

    def turned(u, gain):
        square = u * u
        high = square.astype(jnp.bfloat16)
        rest = (square - high.astype(jnp.float32)).astype(jnp.bfloat16)
        total = jnp.dot(high, block, preferred_element_type=jnp.float32) + jnp.dot(
            rest, block, preferred_element_type=jnp.float32)
        n = u * lax.rsqrt(total * (1.0 / head_dim) + 1e-06) * gain
        quarter = head_dim // 4
        other = jnp.where(left, pltpu.roll(n, LANES - quarter, 1), pltpu.roll(n, quarter, 1))
        return n * cosine + other * sine

    def project(w):
        return jnp.dot(x[...], w, preferred_element_type=jnp.float32).astype(jnp.bfloat16).astype(jnp.float32)

    peak[...] = jnp.full_like(peak, -1e30)
    acc[...] = jnp.zeros_like(acc)

    loads[0].wait()
    pl.semaphore_wait(barrier, n_sp - 1 + n_tp - 1)
    x_copies = []
    for step in range(1, n_tp):
        mine = x.at[own_slice(tp)]
        copy = tp_copy(mine, mine, x_send.at[step], x_recv.at[step], (tp + step) % n_tp)
        copy.start()
        x_copies.append(copy)
    for step in range(1, n_tp):
        theirs = x.at[own_slice((tp + n_tp - step) % n_tp)]
        tp_copy(theirs, theirs, x_send.at[step], x_recv.at[step], (tp + step) % n_tp).wait_recv()

    for i in range(len(wkvs)):
        loads[1 + i].wait()
    if len(wkvs) == 2:
        keys = project(wkvs[0][...])
        vals = project(wkvs[1][...])
        for pair in range(members // 2):
            cut = slice(pair * LANES, (pair + 1) * LANES)
            k, v = turned(keys[:, cut], gain_k), vals[:, cut]
            kv_out[2 * pair] = jnp.where(even, k, pltpu.roll(v, head_dim, 1)).astype(jnp.bfloat16)
            kv_out[2 * pair + 1] = jnp.where(even, pltpu.roll(k, head_dim, 1), v).astype(jnp.bfloat16)
    else:
        both = project(wkvs[0][...])
        kv_out[0] = jnp.where(even, turned(both, gain_k), both).astype(jnp.bfloat16)

    def kv_copy(step):
        to = (sp + step) % n_sp
        return sp_copy(kv_out.at[to % members], kv_all.at[sp], kv_send.at[step], kv_recv.at[sp], to)

    def send_kv(i, carry):
        kv_copy(n_sp - i).start()
        return carry

    lax.fori_loop(1, n_sp, send_kv, 0)
    kv_all[sp] = kv_out[member]

    loads[1 + len(wkvs)].wait()
    for p in range(members):
        u = project(wq[:, p * width:(p + 1) * width])
        for t in range(width // LANES):
            cut = slice(t * LANES, (t + 1) * LANES)
            q_out[p, :, cut] = turned(u[:, cut], gain_q).astype(jnp.bfloat16)

    def q_copy(step):
        to = (member + step) % members
        return sp_copy(q_out.at[to], q_all.at[member], q_send.at[step], q_recv.at[member], first + to)

    for step in range(1, members):
        q_copy(step).start()
    q_all[member] = q_out[member]

    wide_lane = lax.broadcasted_iota(jnp.int32, (rows, width), 1) // head_dim

    def mask_queries(c):
        q = q_all[c]
        for g in range(heads):
            qm[pl.ds(pl.multiple_of((c * heads + g) * rows, rows), rows), :] = jnp.where(
                wide_lane == g, q, jnp.zeros_like(q))

    mask_queries(member)
    for step in range(1, members):
        c = (member + members - step) % members
        sp_copy(q_out.at[c], q_all.at[c], q_send.at[step], q_recv.at[c], first + c).wait_recv()
        mask_queries(c)

    tall = 2 * rows

    def prepare(slot, c):
        tile = kv_all[slot].astype(jnp.float32)
        turned_tile = pltpu.roll(tile, head_dim, 1)
        kk = jnp.where(even, tile, turned_tile).astype(jnp.bfloat16)
        place = pl.ds(c * rows, rows)
        for t in range(width // LANES):
            k4[place, t * LANES:(t + 1) * LANES] = kk
        v1[place, :] = jnp.where(even, turned_tile, 1.0).astype(jnp.bfloat16)

    def wait_kv(slot):
        sp_copy(kv_all.at[slot], kv_all.at[slot], kv_send.at[0], kv_recv.at[slot], sp).wait_recv()

    def attend(c):
        def one(i, carry):
            place = pl.ds(pl.multiple_of(c * heads * rows + i * tall, tall), tall)
            scores = lax.dot_general(qm[place, :], k4[...], (((1,), (1,)), ((), ())),
                                     preferred_element_type=jnp.float32)
            before = peak[place, :]
            now = jnp.maximum(before, jnp.max(scores, axis=1, keepdims=True))
            expo = jnp.exp(scores - jnp.concatenate([now] * (scores.shape[1] // LANES), axis=1))
            peak[place, :] = now
            acc[place, :] = acc[place, :] * jnp.exp(before - now) + jnp.dot(
                expo.astype(jnp.bfloat16), v1[...], preferred_element_type=jnp.float32)
            return carry

        lax.fori_loop(0, heads // 2, one, 0, unroll=True)

    def finish(c):
        parts = []
        for pair in range(heads // 2):
            halves = []
            for g in (2 * pair, 2 * pair + 1):
                piece = acc[pl.ds(pl.multiple_of((c * heads + g) * rows, rows), rows), :]
                halves.append(piece / pltpu.roll(piece, head_dim, 1))
            parts.append(jnp.where(even, halves[0], pltpu.roll(halves[1], head_dim, 1)))
        m_out[c] = jnp.concatenate(parts, axis=1).astype(jnp.bfloat16)

    def m_copy(step):
        to = (member + step) % members
        return sp_copy(m_out.at[to], m_all.at[member], m_send.at[step], m_recv.at[member], first + to)

    for step in range(1, members):
        wait_kv(first + (member + step) % members)
    for c in range(members):
        prepare(first + c, c)

    def whole_group(d, carry):
        base = ((plane + d) % groups) * members

        @pl.when(d > 0)
        def _():
            for c in range(members):
                wait_kv(base + c)
                prepare(base + c, c)

        def per(c, inner):
            attend(c)
            return inner

        lax.fori_loop(0, members, per, 0)
        return carry

    lax.fori_loop(0, groups - 1, whole_group, 0)
    last = ((plane + groups - 1) % groups) * members
    for c in range(members):
        wait_kv(last + c)
        prepare(last + c, c)
    for step in range(1, members + 1):
        c = (member + step) % members
        attend(c)
        finish(c)
        if step < members:
            m_copy(step).start()
    m_all[member] = m_out[member]

    loads[2 + len(wkvs)].wait()
    for step in range(members):
        s = (member + members - step) % members
        if step:
            sp_copy(m_out.at[s], m_all.at[s], m_send.at[step], m_recv.at[s], first + s).wait_recv()
        term = jnp.dot(m_all[s], wo[pl.ds(pl.multiple_of(s * width, width), width), :],
                       preferred_element_type=jnp.float32)
        if step == 0:
            o_acc[...] = term
        else:
            o_acc[...] += term
    o_copies = []
    for step in range(1, n_tp):
        to = (tp + step) % n_tp
        o_out[step] = o_acc[own_slice(to), :].astype(jnp.bfloat16)
        copy = tp_copy(o_out.at[step], o_in.at[step], o_send.at[step], o_recv.at[step], to)
        copy.start()
        o_copies.append(copy)
    result = o_acc[own_slice(tp), :].astype(jnp.bfloat16).astype(jnp.float32)
    for step in range(1, n_tp):
        o_copies[step - 1].wait_recv()
        result = result + o_in[step].astype(jnp.float32)
    out_ref[...] = result.astype(jnp.bfloat16)

    for copy in x_copies + o_copies:
        copy.wait_send()
    for step in range(1, members):
        q_copy(step).wait_send()
        m_copy(step).wait_send()

    def sent_kv(step, carry):
        kv_copy(step).wait_send()
        return carry

    lax.fori_loop(1, n_sp, sent_kv, 0)


def solution(mesh):
    n_sp, n_tp = mesh.shape["sp"], mesh.shape["tp"]

    def body(tokens_in, w_query, w_key, w_value, w_out, q_gain, k_gain):
        head_dim = q_gain.shape[0]
        own_rows, depth = tokens_in.shape
        rows = own_rows * n_tp
        query_cols, key_cols = w_query.shape[1], w_key.shape[1]
        members = key_cols // head_dim
        width = query_cols // members
        heads = width // head_dim
        if key_cols % LANES:
            wkv = (jnp.concatenate([w_key, w_value], axis=1),)
        else:
            wkv = (w_key, w_value)
        row_table, col_table = tables(rows * n_sp, head_dim)
        bf, f32 = jnp.bfloat16, jnp.float32
        hbm = pl.BlockSpec(memory_space=pltpu.HBM)
        vmem = pl.BlockSpec(memory_space=pltpu.VMEM)
        dma = pltpu.SemaphoreType.DMA
        call = pl.pallas_call(
            functools.partial(kernel, n_sp, n_tp, members, head_dim),
            out_shape=jax.ShapeDtypeStruct((own_rows, w_out.shape[1]), bf),
            in_specs=[hbm, hbm, (hbm,) * len(wkv), hbm, vmem, vmem, vmem, vmem],
            out_specs=vmem,
            scratch_shapes=[
                pltpu.VMEM((rows, depth), bf),
                pltpu.VMEM(w_query.shape, bf),
                tuple(pltpu.VMEM(w.shape, bf) for w in wkv),
                pltpu.VMEM(w_out.shape, bf),
                pltpu.VMEM((members, rows, LANES), bf),
                pltpu.VMEM((n_sp, rows, LANES), bf),
                pltpu.VMEM((members, rows, width), bf),
                pltpu.VMEM((members, rows, width), bf),
                pltpu.VMEM((members * heads * rows, width), bf),
                pltpu.VMEM((members * rows, width), bf),
                pltpu.VMEM((members * rows, LANES), bf),
                pltpu.VMEM((members * heads * rows, LANES), f32),
                pltpu.VMEM((members * heads * rows, LANES), f32),
                pltpu.VMEM((members, rows, width), bf),
                pltpu.VMEM((members, rows, width), bf),
                pltpu.VMEM((rows, w_out.shape[1]), f32),
                pltpu.VMEM((n_tp, own_rows, w_out.shape[1]), bf),
                pltpu.VMEM((n_tp, own_rows, w_out.shape[1]), bf),
                dma((6,)),
                dma((n_tp,)), dma((n_tp,)),
                dma((n_sp,)), dma((n_sp,)),
                dma((members,)), dma((members,)),
                dma((members,)), dma((members,)),
                dma((n_tp,)), dma((n_tp,)),
            ],
            compiler_params=pltpu.CompilerParams(
                collective_id=0, has_side_effects=True, vmem_limit_bytes=56 * 1024 * 1024),
        )
        return call(tokens_in, w_query, wkv, w_out, jnp.asarray(row_table), jnp.asarray(col_table),
                    q_gain.reshape(1, head_dim), k_gain.reshape(1, head_dim))

    return jax.shard_map(
        body,
        mesh=mesh,
        in_specs=(
            P(("sp", "tp"), None),
            P(None, "tp"),
            P(None, "tp"),
            P(None, "tp"),
            P("tp", None),
            P(),
            P(),
        ),
        out_specs=P(("sp", "tp"), None),
        check_vma=False,
    )
```

time: 118 us -> 40.8 us (0.35)
  waiting for transfers between devices: 70.1 us -> 0 us
  Pallas kernels: 0 us -> 38.4 us
  matrix products: 19.1 us -> 0 us
  between operations: 13.6 us -> 0.01 us
  other arithmetic: 9.04 us -> 0 us
  blocking collectives: 2.5 us -> 0 us
  local copies, waits for them, and re-layouts: 3.27 us -> 1.67 us
    all_gather x1 -> x0, waiting for transfers between devices: 63.8 us -> none  [body(): piece = lax.all_gather(outgoing, 'sp', axis=0, tiled=True)]
    pallas_call x0 -> x1, Pallas kernels: none -> 38.4 us  [body(): call(tokens_in, w_query, wkv, w_out, jnp.asarray(row_table), jnp.asarray(...]
    dot_general x4 -> x0, matrix products: 19.1 us -> none  [the longest x1 8.83 us: body(): jnp.einsum('kgqn,nkd->kgqd', expo.astype(jnp.bfloat16), piece[:, key_cols...]
    reduce_scatter x1 -> x0, waiting for transfers between devices: 6.26 us -> none  [body(): lax.psum_scatter(jnp.dot(mixed, w_out, preferred_element_type=jnp.float32...]
    reduce_sum x3 -> x0, other arithmetic: 4.84 us -> none  [the longest x1 3.27 us: body(): total = jnp.sum(expo, axis=-1)]
    all_gather x1 -> x0, blocking collectives: 2.5 us -> none  [body(): lax.all_gather(tokens_in, 'tp', axis=0, tiled=True)]
    convert_element_type x4 -> x0, other arithmetic: 1.9 us -> none  [the longest x1 1.84 us: body(): piece[:, :key_cols].astype(jnp.float32).reshape(length, kv_heads, head_dim)]
    unnamed x6 -> x1, local copies, waits for them, and re-layouts: 2.44 us -> 1.67 us
  transfers between devices with their start and end apart: 2 -> 0, of which waited for: 2 -> 0; matrix products, arithmetic and copies ran while one was open for 1% -> 0% of each run, Pallas kernels for 0% -> 0%
where the time goes in v1:
time: 40.8 us; the launch traced here: 40 us
  Pallas kernels  38.4 us (94%)
  local copies, waits for them, and re-layouts  1.67 us (4%)
    pallas_call x1, Pallas kernels, body(): call(tokens_in, w_query, wkv, w_out, jnp.asarray(row_table), jnp.asarray(...  38.4 us
    unnamed x1, local copies, waits for them, and re-layouts  1.67 us

profile of v1, /device:TPU:0, one launch (start us, length us, event | category | flops | bytes accessed | tf_op | source)
XLA Modules:
  0.0 40.0 jit_solution(438251563819441712)
XLA Ops:
  0.0 38.4 %shard_map.91 = bf16[64,2048]{1,0:T(8,128)(2,1)} custom-call(bf16[64,2048]{1,0:T(8,128)(2,1)} %tok_hbm.1, bf16[2048,1024]{1,0:T(8,128)(2,1)} %wq_hbm.1, bf16[2048,256]{1,0:T(8,128)(2,1)} %wkv_hbms_0_.1, bf16[2048,256]{1,0:T(8,128)(2,1)} %wkv_hbms_1_.1, bf16[1024,2048]{1,0:T(8,128)(2,1)} %wo_hbm.1, f32[32,256]{1,0:T(8,128)} %constant.4.clone.row_ref, ...), custom_call_target="tpu_custom_call" | custom-call | tf_op jit(solution)/shard_map/pallas_call | solution.py:342
  38.4 1.7 %copy.11 = bf16[64,2048]{1,0:T(8,128)(2,1)} copy(bf16[64,2048]{1,0:T(8,128)(2,1)} %shard_map.91) | data formatting | bytes 524288

commit v2 on v1

--- a/solution.py
+++ b/solution.py
@@ -29,7 +29,7 @@
     n_sp, n_tp, members, head_dim,
     tok_hbm, wq_hbm, wkv_hbms, wo_hbm, row_ref, col_ref, qg_ref, kg_ref, out_ref,
     x, wq, wkvs, wo, kv_out, kv_all, q_out, q_all, qm, k4, v1, peak, acc, m_out, m_all, o_acc, o_out, o_in,
-    load_sem, x_send, x_recv, kv_send, kv_recv, q_send, q_recv, m_send, m_recv, o_send, o_recv,
+    load_sem, x_send, x_recv, kv_send, kv_recv, line_send, q_send, q_recv, m_send, m_recv, o_send, o_recv,
 ):
     sp, tp = lax.axis_index("sp"), lax.axis_index("tp")
     own_rows = tok_hbm.shape[0]
@@ -63,11 +63,16 @@
     for step in range(1, n_tp):
         pl.semaphore_signal(barrier, inc=1, device_id={"tp": (tp + step) % n_tp}, device_id_type=pl.DeviceIdType.MESH)
 
+    for step in range(1, members):
+        pl.semaphore_signal(barrier, inc=1, device_id={"sp": first + (member + step) % members},
+                            device_id_type=pl.DeviceIdType.MESH)
+
     def greet(step, carry):
-        pl.semaphore_signal(barrier, inc=1, device_id={"sp": (sp + step) % n_sp}, device_id_type=pl.DeviceIdType.MESH)
+        pl.semaphore_signal(barrier, inc=1, device_id={"sp": (sp + step * members) % n_sp},
+                            device_id_type=pl.DeviceIdType.MESH)
         return carry
 
-    lax.fori_loop(1, n_sp, greet, 0)
+    lax.fori_loop(1, groups, greet, 0)
 
     lane = lax.broadcasted_iota(jnp.int32, (rows, LANES), 1)
     low = lane % head_dim < head_dim // 2
@@ -106,7 +111,7 @@
     acc[...] = jnp.zeros_like(acc)
 
     loads[0].wait()
-    pl.semaphore_wait(barrier, n_sp - 1 + n_tp - 1)
+    pl.semaphore_wait(barrier, groups - 1 + members - 1 + n_tp - 1)
     x_copies = []
     for step in range(1, n_tp):
         mine = x.at[own_slice(tp)]
@@ -131,16 +136,29 @@
         both = project(wkvs[0][...])
         kv_out[0] = jnp.where(even, turned(both, gain_k), both).astype(jnp.bfloat16)
 
+    kv_all[sp] = kv_out[member]
+
     def kv_copy(step):
-        to = (sp + step) % n_sp
-        return sp_copy(kv_out.at[to % members], kv_all.at[sp], kv_send.at[step], kv_recv.at[sp], to)
-
-    def send_kv(i, carry):
-        kv_copy(n_sp - i).start()
-        return carry
-
-    lax.fori_loop(1, n_sp, send_kv, 0)
-    kv_all[sp] = kv_out[member]
+        to = (member + step) % members
+        return sp_copy(kv_out.at[to], kv_all.at[sp], kv_send.at[step], kv_recv.at[sp], first + to)
+
+    for step in range(1, members):
+        kv_copy(step).start()
+
+    below, above = plane, groups - 1 - plane
+    both_sides = jnp.minimum(below, above)
+
+    def nearest(i):
+        distance = jnp.where(i <= 2 * both_sides, (i + 1) // 2, i - both_sides)
+        upward = jnp.where(i <= 2 * both_sides, i % 2, jnp.where(above > below, 1, 0))
+        return plane + distance * (2 * upward - 1)
+
+    def line_copy(i, c):
+        slot = kv_all.at[first + c]
+        return sp_copy(slot, slot, line_send.at[i * members + c], kv_recv.at[first + c], nearest(i) * members + member)
+
+    def wait_kv(slot):
+        sp_copy(kv_all.at[slot], kv_all.at[slot], kv_send.at[0], kv_recv.at[slot], sp).wait_recv()
 
     loads[1 + len(wkvs)].wait()
     for p in range(members):
@@ -157,6 +175,16 @@
         q_copy(step).start()
     q_all[member] = q_out[member]
 
+    for step in range(1, members):
+        wait_kv(first + (member + members - step) % members)
+
+    def along(i, carry):
+        for c in range(members):
+            line_copy(i, c).start()
+        return carry
+
+    lax.fori_loop(1, groups, along, 0)
+
     wide_lane = lax.broadcasted_iota(jnp.int32, (rows, width), 1) // head_dim
 
     def mask_queries(c):
@@ -165,13 +193,7 @@
             qm[pl.ds(pl.multiple_of((c * heads + g) * rows, rows), rows), :] = jnp.where(
                 wide_lane == g, q, jnp.zeros_like(q))
 
-    mask_queries(member)
-    for step in range(1, members):
-        c = (member + members - step) % members
-        sp_copy(q_out.at[c], q_all.at[c], q_send.at[step], q_recv.at[c], first + c).wait_recv()
-        mask_queries(c)
-
-    tall = 2 * rows
+    tall = heads * rows
 
     def prepare(slot, c):
         tile = kv_all[slot].astype(jnp.float32)
@@ -182,23 +204,16 @@
             k4[place, t * LANES:(t + 1) * LANES] = kk
         v1[place, :] = jnp.where(even, turned_tile, 1.0).astype(jnp.bfloat16)
 
-    def wait_kv(slot):
-        sp_copy(kv_all.at[slot], kv_all.at[slot], kv_send.at[0], kv_recv.at[slot], sp).wait_recv()
-
     def attend(c):
-        def one(i, carry):
-            place = pl.ds(pl.multiple_of(c * heads * rows + i * tall, tall), tall)
-            scores = lax.dot_general(qm[place, :], k4[...], (((1,), (1,)), ((), ())),
-                                     preferred_element_type=jnp.float32)
-            before = peak[place, :]
-            now = jnp.maximum(before, jnp.max(scores, axis=1, keepdims=True))
-            expo = jnp.exp(scores - jnp.concatenate([now] * (scores.shape[1] // LANES), axis=1))
-            peak[place, :] = now
-            acc[place, :] = acc[place, :] * jnp.exp(before - now) + jnp.dot(
-                expo.astype(jnp.bfloat16), v1[...], preferred_element_type=jnp.float32)
-            return carry
-
-        lax.fori_loop(0, heads // 2, one, 0, unroll=True)
+        place = pl.ds(pl.multiple_of(c * tall, tall), tall)
+        scores = lax.dot_general(qm[place, :], k4[...], (((1,), (1,)), ((), ())),
+                                 preferred_element_type=jnp.float32)
+        before = peak[place, :]
+        now = jnp.maximum(before, jnp.max(scores, axis=1, keepdims=True))
+        expo = jnp.exp(scores - jnp.concatenate([now] * (scores.shape[1] // LANES), axis=1))
+        peak[place, :] = now
+        acc[place, :] = acc[place, :] * jnp.exp(before - now) + jnp.dot(
+            expo.astype(jnp.bfloat16), v1[...], preferred_element_type=jnp.float32)
 
     def finish(c):
         parts = []
@@ -214,32 +229,29 @@
         to = (member + step) % members
         return sp_copy(m_out.at[to], m_all.at[member], m_send.at[step], m_recv.at[member], first + to)
 
-    for step in range(1, members):
-        wait_kv(first + (member + step) % members)
     for c in range(members):
         prepare(first + c, c)
-
-    def whole_group(d, carry):
-        base = ((plane + d) % groups) * members
-
-        @pl.when(d > 0)
-        def _():
-            for c in range(members):
-                wait_kv(base + c)
-                prepare(base + c, c)
-
-        def per(c, inner):
+    for step in range(members):
+        c = (member + members - step) % members
+        if step:
+            sp_copy(q_out.at[c], q_all.at[c], q_send.at[step], q_recv.at[c], first + c).wait_recv()
+        mask_queries(c)
+        attend(c)
+
+    def fetch(i):
+        base = nearest(i) * members
+        for c in range(members):
+            wait_kv(base + c)
+            prepare(base + c, c)
+
+    def whole_group(i, carry):
+        fetch(i)
+        for c in range(members):
             attend(c)
-            return inner
-
-        lax.fori_loop(0, members, per, 0)
         return carry
 
-    lax.fori_loop(0, groups - 1, whole_group, 0)
-    last = ((plane + groups - 1) % groups) * members
-    for c in range(members):
-        wait_kv(last + c)
-        prepare(last + c, c)
+    lax.fori_loop(1, groups - 1, whole_group, 0)
+    fetch(groups - 1)
     for step in range(1, members + 1):
         c = (member + step) % members
         attend(c)
@@ -275,14 +287,16 @@
     for copy in x_copies + o_copies:
         copy.wait_send()
     for step in range(1, members):
+        kv_copy(step).wait_send()
         q_copy(step).wait_send()
         m_copy(step).wait_send()
 
-    def sent_kv(step, carry):
-        kv_copy(step).wait_send()
+    def sent_along(i, carry):
+        for c in range(members):
+            line_copy(i, c).wait_send()
         return carry
 
-    lax.fori_loop(1, n_sp, sent_kv, 0)
+    lax.fori_loop(1, groups, sent_along, 0)
 
 
 def solution(mesh):
@@ -331,7 +345,7 @@
                 pltpu.VMEM((n_tp, own_rows, w_out.shape[1]), bf),
                 dma((6,)),
                 dma((n_tp,)), dma((n_tp,)),
-                dma((n_sp,)), dma((n_sp,)),
+                dma((members,)), dma((n_sp,)), dma((n_sp,)),
                 dma((members,)), dma((members,)),
                 dma((members,)), dma((members,)),
                 dma((n_tp,)), dma((n_tp,)),

time: 40.8 us -> 37.5 us (0.919); the launches traced: 40 us -> 37.3 us
  Pallas kernels: 38.4 us -> 35.6 us
    pallas_call x1, Pallas kernels: 38.4 us -> 35.6 us  [body(): call(tokens_in, w_query, wkv, w_out, jnp.asarray(row_table), jnp.asarray(...]
where the time goes in v2:
time: 37.5 us; the launch traced here: 37.3 us
  Pallas kernels  35.6 us (95%)
  local copies, waits for them, and re-layouts  1.67 us (4%)
    pallas_call x1, Pallas kernels, body(): call(tokens_in, w_query, wkv, w_out, jnp.asarray(row_table), jnp.asarray(...  35.6 us
    unnamed x1, local copies, waits for them, and re-layouts  1.67 us

profile of v2, /device:TPU:0, one launch (start us, length us, event | category | flops | bytes accessed | tf_op | source)
XLA Modules:
  0.0 37.3 jit_solution(13134338027527948860)
XLA Ops:
  0.0 35.6 %shard_map.91 = bf16[64,2048]{1,0:T(8,128)(2,1)} custom-call(bf16[64,2048]{1,0:T(8,128)(2,1)} %tok_hbm.1, bf16[2048,1024]{1,0:T(8,128)(2,1)} %wq_hbm.1, bf16[2048,256]{1,0:T(8,128)(2,1)} %wkv_hbms_0_.1, bf16[2048,256]{1,0:T(8,128)(2,1)} %wkv_hbms_1_.1, bf16[1024,2048]{1,0:T(8,128)(2,1)} %wo_hbm.1, f32[32,256]{1,0:T(8,128)} %constant.4.clone.row_ref, ...), custom_call_target="tpu_custom_call" | custom-call | tf_op jit(solution)/shard_map/pallas_call | solution.py:356
  35.6 1.7 %copy.11 = bf16[64,2048]{1,0:T(8,128)(2,1)} copy(bf16[64,2048]{1,0:T(8,128)(2,1)} %shard_map.91) | data formatting | bytes 524288

commit v3 on v2

--- a/solution.py
+++ b/solution.py
@@ -10,6 +10,7 @@
 
 GRID_W = 64
 LANES = 128
+REACH = 2
 
 
 def tables(token_count, head_dim):
@@ -29,7 +30,7 @@
     n_sp, n_tp, members, head_dim,
     tok_hbm, wq_hbm, wkv_hbms, wo_hbm, row_ref, col_ref, qg_ref, kg_ref, out_ref,
     x, wq, wkvs, wo, kv_out, kv_all, q_out, q_all, qm, k4, v1, peak, acc, m_out, m_all, o_acc, o_out, o_in,
-    load_sem, x_send, x_recv, kv_send, kv_recv, line_send, q_send, q_recv, m_send, m_recv, o_send, o_recv,
+    load_sem, x_send, x_recv, kv_send, kv_recv, line_send, on_send, q_send, q_recv, m_send, m_recv, o_send, o_recv,
 ):
     sp, tp = lax.axis_index("sp"), lax.axis_index("tp")
     own_rows = tok_hbm.shape[0]
@@ -54,6 +55,19 @@
     def own_slice(index):
         return pl.ds(pl.multiple_of(index * own_rows, own_rows), own_rows)
 
+    below, above = plane, groups - 1 - plane
+    both_sides = jnp.minimum(below, above)
+
+    def way(i):
+        paired = i <= 2 * both_sides
+        distance = jnp.where(paired, (i + 1) // 2, i - both_sides)
+        upward = jnp.where(paired, i % 2, jnp.where(above > below, 1, 0))
+        return distance, 2 * upward - 1
+
+    def nearest(i):
+        distance, side = way(i)
+        return plane + distance * side
+
     loads = [pltpu.make_async_copy(tok_hbm, x.at[own_slice(tp)], load_sem.at[0])]
     for i, (src, dst) in enumerate(zip((*wkv_hbms, wq_hbm, wo_hbm), (*wkvs, wq, wo))):
         loads.append(pltpu.make_async_copy(src, dst, load_sem.at[i + 1]))
@@ -67,9 +81,11 @@
         pl.semaphore_signal(barrier, inc=1, device_id={"sp": first + (member + step) % members},
                             device_id_type=pl.DeviceIdType.MESH)
 
-    def greet(step, carry):
-        pl.semaphore_signal(barrier, inc=1, device_id={"sp": (sp + step * members) % n_sp},
-                            device_id_type=pl.DeviceIdType.MESH)
+    def greet(i, carry):
+        @pl.when(way(i)[0] <= REACH)
+        def _():
+            pl.semaphore_signal(barrier, inc=1, device_id={"sp": nearest(i) * members + member},
+                                device_id_type=pl.DeviceIdType.MESH)
         return carry
 
     lax.fori_loop(1, groups, greet, 0)
@@ -111,7 +127,8 @@
     acc[...] = jnp.zeros_like(acc)
 
     loads[0].wait()
-    pl.semaphore_wait(barrier, groups - 1 + members - 1 + n_tp - 1)
+    pl.semaphore_wait(
+        barrier, jnp.minimum(below, REACH) + jnp.minimum(above, REACH) + members - 1 + n_tp - 1)
     x_copies = []
     for step in range(1, n_tp):
         mine = x.at[own_slice(tp)]
@@ -145,17 +162,30 @@
     for step in range(1, members):
         kv_copy(step).start()
 
-    below, above = plane, groups - 1 - plane
-    both_sides = jnp.minimum(below, above)
-
-    def nearest(i):
-        distance = jnp.where(i <= 2 * both_sides, (i + 1) // 2, i - both_sides)
-        upward = jnp.where(i <= 2 * both_sides, i % 2, jnp.where(above > below, 1, 0))
-        return plane + distance * (2 * upward - 1)
-
     def line_copy(i, c):
         slot = kv_all.at[first + c]
         return sp_copy(slot, slot, line_send.at[i * members + c], kv_recv.at[first + c], nearest(i) * members + member)
+
+    def onward(i, act):
+        distance, side = way(i)
+
+        @pl.when((distance >= REACH) & (plane - side >= 0) & (plane - side < groups))
+        def _():
+            for c in range(members):
+                slot = (plane + distance * side) * members + c
+                act(sp_copy(kv_all.at[slot], kv_all.at[slot], on_send.at[i * members + c], kv_recv.at[slot],
+                            (plane - side) * members + member))
+
+    def along(step):
+        def one(i, carry):
+            @pl.when(way(i)[0] <= REACH)
+            def _():
+                line_copy(i, (member + step) % members).start()
+            return carry
+
+        lax.fori_loop(1, groups, one, 0)
+
+    along(0)
 
     def wait_kv(slot):
         sp_copy(kv_all.at[slot], kv_all.at[slot], kv_send.at[0], kv_recv.at[slot], sp).wait_recv()
@@ -177,13 +207,7 @@
 
     for step in range(1, members):
         wait_kv(first + (member + members - step) % members)
-
-    def along(i, carry):
-        for c in range(members):
-            line_copy(i, c).start()
-        return carry
-
-    lax.fori_loop(1, groups, along, 0)
+        along(members - step)
 
     wide_lane = lax.broadcasted_iota(jnp.int32, (rows, width), 1) // head_dim
 
@@ -242,6 +266,8 @@
         base = nearest(i) * members
         for c in range(members):
             wait_kv(base + c)
+        onward(i, lambda copy: copy.start())
+        for c in range(members):
             prepare(base + c, c)
 
     def whole_group(i, carry):
@@ -292,8 +318,12 @@
         m_copy(step).wait_send()
 
     def sent_along(i, carry):
-        for c in range(members):
-            line_copy(i, c).wait_send()
+        @pl.when(way(i)[0] <= REACH)
+        def _():
+            for c in range(members):
+                line_copy(i, c).wait_send()
+
+        onward(i, lambda copy: copy.wait_send())
         return carry
 
     lax.fori_loop(1, groups, sent_along, 0)
@@ -345,7 +375,7 @@
                 pltpu.VMEM((n_tp, own_rows, w_out.shape[1]), bf),
                 dma((6,)),
                 dma((n_tp,)), dma((n_tp,)),
-                dma((members,)), dma((n_sp,)), dma((n_sp,)),
+                dma((members,)), dma((n_sp,)), dma((n_sp,)), dma((n_sp,)),
                 dma((members,)), dma((members,)),
                 dma((members,)), dma((members,)),
                 dma((n_tp,)), dma((n_tp,)),

time: 37.5 us -> 37.5 us (level)
  no operation moved by 1% of the time
where the time goes in v3:
time: 37.5 us; the launch traced here: 37.3 us
  Pallas kernels  35.6 us (95%)
  local copies, waits for them, and re-layouts  1.67 us (4%)
    pallas_call x1, Pallas kernels, body(): call(tokens_in, w_query, wkv, w_out, jnp.asarray(row_table), jnp.asarray(...  35.6 us
    unnamed x1, local copies, waits for them, and re-layouts  1.67 us

profile of v3, /device:TPU:0, one launch (start us, length us, event | category | flops | bytes accessed | tf_op | source)
XLA Modules:
  0.0 37.3 jit_solution(15394347210698967227)
XLA Ops:
  0.0 35.6 %shard_map.91 = bf16[64,2048]{1,0:T(8,128)(2,1)} custom-call(bf16[64,2048]{1,0:T(8,128)(2,1)} %tok_hbm.1, bf16[2048,1024]{1,0:T(8,128)(2,1)} %wq_hbm.1, bf16[2048,256]{1,0:T(8,128)(2,1)} %wkv_hbms_0_.1, bf16[2048,256]{1,0:T(8,128)(2,1)} %wkv_hbms_1_.1, bf16[1024,2048]{1,0:T(8,128)(2,1)} %wo_hbm.1, f32[32,256]{1,0:T(8,128)} %constant.4.clone.row_ref, ...), custom_call_target="tpu_custom_call" | custom-call | tf_op jit(solution)/shard_map/pallas_call | solution.py:386
  35.6 1.7 %copy.11 = bf16[64,2048]{1,0:T(8,128)(2,1)} copy(bf16[64,2048]{1,0:T(8,128)(2,1)} %shard_map.91) | data formatting | bytes 524288

commit v4 on v3

--- a/solution.py
+++ b/solution.py
@@ -10,7 +10,7 @@
 
 GRID_W = 64
 LANES = 128
-REACH = 2
+REACH = 1 << 20
 
 
 def tables(token_count, head_dim):

time: 37.5 us -> 34.2 us (0.912)
  Pallas kernels: 35.6 us -> 32.3 us
    pallas_call x1, Pallas kernels: 35.6 us -> 32.3 us  [body(): call(tokens_in, w_query, wkv, w_out, jnp.asarray(row_table), jnp.asarray(...]
where the time goes in v4:
time: 34.2 us; the launch traced here: 34 us
  Pallas kernels  32.3 us (94%)
  local copies, waits for them, and re-layouts  1.67 us (5%)
    pallas_call x1, Pallas kernels, body(): call(tokens_in, w_query, wkv, w_out, jnp.asarray(row_table), jnp.asarray(...  32.3 us
    unnamed x1, local copies, waits for them, and re-layouts  1.67 us

profile of v4, /device:TPU:0, one launch (start us, length us, event | category | flops | bytes accessed | tf_op | source)
XLA Modules:
  0.0 34.0 jit_solution(5752604101866483028)
XLA Ops:
  0.0 32.3 %shard_map.91 = bf16[64,2048]{1,0:T(8,128)(2,1)} custom-call(bf16[64,2048]{1,0:T(8,128)(2,1)} %tok_hbm.1, bf16[2048,1024]{1,0:T(8,128)(2,1)} %wq_hbm.1, bf16[2048,256]{1,0:T(8,128)(2,1)} %wkv_hbms_0_.1, bf16[2048,256]{1,0:T(8,128)(2,1)} %wkv_hbms_1_.1, bf16[1024,2048]{1,0:T(8,128)(2,1)} %wo_hbm.1, f32[32,256]{1,0:T(8,128)} %constant.4.clone.row_ref, ...), custom_call_target="tpu_custom_call" | custom-call | tf_op jit(solution)/shard_map/pallas_call | solution.py:386
  32.3 1.7 %copy.11 = bf16[64,2048]{1,0:T(8,128)(2,1)} copy(bf16[64,2048]{1,0:T(8,128)(2,1)} %shard_map.91) | data formatting | bytes 524288
